TPU v7x, 32 devices: a whole 2x2x4 slice. The times are simulated.
32 devices in a mesh: ep: 16 (over z, y, x), tp: 2 (over core).
Axes of the slice: x: 2, y: 2, z: 4, core: 2. Of those that a mesh axis runs over, the one named last changes fastest.
Arguments:
- tokens: bfloat16 [128, 2048], P('ep'), may hold values from -6 to 6
- mixer_norm_gain: float32 [2048], replicated, may hold values from 0.1 to 1.9
- gate_projection_weight: bfloat16 [2048, 2, 2048], P(None, 'tp', 'ep'), may hold values from -0.125 to 0.125
- value_projection_weight: bfloat16 [2048, 2, 2048], P(None, 'tp', 'ep'), may hold values from -0.125 to 0.125
- input_projection_weight: bfloat16 [2048, 1024], P(None, 'tp'), may hold values from -0.125 to 0.125
- output_projection_weight: bfloat16 [2048, 1024], P(None, 'tp'), may hold values from -0.125 to 0.125
- step_projection_weight: bfloat16 [2048, 64], P(None, 'tp'), may hold values from -0.125 to 0.125
- head_step_bias: float32 [64], P('tp'), may hold values from -1 to 1
- head_decay_rate: float32 [64], P('tp'), may hold values from 0.02 to 3
- extra_log_decay: float32 [128, 64], P('ep', 'tp'), may hold values from -0.7 to 0
- value_taps: float32 [4, 4096], P(None, 'tp'), may hold values from -3 to 3
- input_taps: float32 [4, 1024], P(None, 'tp'), may hold values from -3 to 3
- output_taps: float32 [4, 1024], P(None, 'tp'), may hold values from -3 to 3
- prior_values: bfloat16 [128, 3, 4096], P('ep', None, 'tp'), may hold values from -6 to 6
- prior_input_maps: bfloat16 [128, 3, 1024], P('ep', None, 'tp'), may hold values from -6 to 6
- prior_output_maps: bfloat16 [128, 3, 1024], P('ep', None, 'tp'), may hold values from -6 to 6
- head_skip_gain: float32 [64], P('tp'), may hold values from 0.5 to 1.5
- group_norm_gain: float32 [4096], P('tp'), may hold values from 0.1 to 1.9
- mixer_output_weight: bfloat16 [4096, 2048], P('tp', 'ep'), may hold values from -0.09375 to 0.09375
- recurrent_state: float32 [128, 64, 64, 128], P('ep', 'tp'), may hold values from -6 to 6
- expert_norm_gain: float32 [2048], replicated, may hold values from 0.1 to 1.9
- routes: int32 [128, 6], P('ep'), may hold values from 0 to 15, all different within a row; in each aligned block of 8 rows (0 to 7, 8 to 15, ...) at most 4 rows name the same one
- chosen_expert_weight: float32 [128, 6], P('ep'), may hold values from 0.2 to 1
- routed_gate_weight: bfloat16 [16, 2048, 512], P('ep', None, 'tp'), may hold values from -0.125 to 0.125
- routed_up_weight: bfloat16 [16, 2048, 512], P('ep', None, 'tp'), may hold values from -0.125 to 0.125
- routed_down_weight: bfloat16 [16, 512, 2048], P('ep', 'tp'), may hold values from -0.25 to 0.25
- common_gate_weight: bfloat16 [2048, 512], P(None, 'tp'), may hold values from -0.125 to 0.125
- common_up_weight: bfloat16 [2048, 512], P(None, 'tp'), may hold values from -0.125 to 0.125
- common_down_weight: bfloat16 [512, 2048], P('tp'), may hold values from -0.25 to 0.25
Outputs:
- result: bfloat16 [128, 2048], P('ep')
- state_next: float32 [128, 64, 64, 128], P('ep', 'tp')
- next_value: bfloat16 [128, 3, 4096], P('ep', None, 'tp')
- next_input: bfloat16 [128, 3, 1024], P('ep', None, 'tp')
- next_output: bfloat16 [128, 3, 1024], P('ep', None, 'tp')
Inputs may be any that keep to these rules, and one draw needn't show every extreme that they name: `routes`: the 6 experts of a row differ; among the rows of one device (aligned blocks of 8 rows) no expert is named more than 4 times.
All inputs are finite; a program needn't handle non-finite values.
Results may differ from a plain program's by a relative error of at most 0.015.
Values may be sent and summed in bfloat16 or wider, within the bound.
No kernel may reach another device: no remote copies, remote signals or barrier semaphores. Data moves between devices by JAX's collectives and lax.ppermute only.
A program may use at most 128 MiB of HBM per device.

v0:
```python
import jax
import jax.numpy as jnp
from jax import lax
from jax.sharding import PartitionSpec as P

D_INNER = 4096
GROUPS = 8


EPSILON = 1e-06


def rms_scale(values, gain_vec):
    values = values.astype(jnp.float32)
    return (
        values * lax.rsqrt(jnp.mean(values * values, axis=-1, keepdims=True) + EPSILON) * gain_vec
    )


def short_conv(past_rows, fresh_row, weight):
    window = jnp.concatenate([past_rows, fresh_row[:, None, :]], axis=1)
    summed = window[:, 0].astype(jnp.float32) * weight[0]
    for offset in range(1, window.shape[1]):
        summed = summed + window[:, offset].astype(jnp.float32) * weight[offset]
    return (jax.nn.silu(summed), window[:, 1:])


def state_step(
    state_prev, value_conv, input_conv, output_conv, timestep_size, step_decay, head_skip_gain
):
    batch_rows, head_count, head_size, state_size = state_prev.shape
    per_group = head_count // (input_conv.shape[1] // state_size)
    value_heads = value_conv.reshape(batch_rows, head_count, head_size)
    input_heads = jnp.repeat(input_conv.reshape(batch_rows, -1, state_size), per_group, axis=1)
    output_heads = jnp.repeat(output_conv.reshape(batch_rows, -1, state_size), per_group, axis=1)
    state_next = (
        step_decay[:, :, None, None] * state_prev
        + (timestep_size[:, :, None] * value_heads)[:, :, :, None] * input_heads[:, :, None, :]
    )
    mixed_heads = (
        jnp.sum(state_next * output_heads[:, :, None, :], axis=-1)
        + head_skip_gain[None, :, None] * value_heads
    )
    return (state_next, mixed_heads.reshape(batch_rows, -1))


def gated_norm(mixed_flat, gate_rows, group_norm_gain, group_width):
    gated_rows = mixed_flat * jax.nn.silu(gate_rows.astype(jnp.float32))
    grouped = gated_rows.reshape(gated_rows.shape[0], -1, group_width)
    grouped = grouped * lax.rsqrt(jnp.mean(grouped * grouped, axis=-1, keepdims=True) + EPSILON)
    return (grouped.reshape(gated_rows.shape[0], -1) * group_norm_gain).astype(jnp.bfloat16)


def expert_partial(arrived, gate_mat, up_mat, down_mat):
    gate_part = jnp.einsum("slcd,ldf->slcf", arrived, gate_mat, preferred_element_type=jnp.float32)
    up_part = jnp.einsum("slcd,ldf->slcf", arrived, up_mat, preferred_element_type=jnp.float32)
    hidden = (jax.nn.silu(gate_part) * up_part).astype(jnp.bfloat16)
    return jnp.einsum("slcf,lfd->slcd", hidden, down_mat, preferred_element_type=jnp.float32)


def shards(
    tokens,
    mixer_norm_gain,
    gate_projection_weight,
    value_projection_weight,
    input_projection_weight,
    output_projection_weight,
    step_projection_weight,
    head_step_bias,
    head_decay_rate,
    extra_log_decay,
    value_taps,
    input_taps,
    output_taps,
    prior_values,
    prior_input_maps,
    prior_output_maps,
    head_skip_gain,
    group_norm_gain,
    mixer_output_weight,
    recurrent_state,
    expert_norm_gain,
    routes,
    chosen_expert_weight,
    routed_gate_weight,
    routed_up_weight,
    routed_down_weight,
    common_gate_weight,
    common_up_weight,
    common_down_weight,
):
    seq_rows, model_width = tokens.shape
    ep_count = lax.axis_size("ep")
    tp_count = lax.axis_size("tp")
    tp_place = lax.axis_index("tp")
    normed = rms_scale(tokens, mixer_norm_gain).astype(jnp.bfloat16)
    both_pieces = jnp.concatenate(
        [
            gate_projection_weight.reshape(model_width, -1),
            value_projection_weight.reshape(model_width, -1),
        ],
        axis=1,
    )
    piece_width = both_pieces.shape[1] // 2
    projected = jnp.dot(
        lax.all_gather(normed, "ep", axis=0, tiled=True),
        both_pieces,
        preferred_element_type=jnp.float32,
    ).astype(jnp.bfloat16)
    returned = lax.all_to_all(projected, "ep", split_axis=0, concat_axis=1, tiled=True).reshape(
        seq_rows, ep_count, 2, piece_width
    )
    gate_rows = returned[:, :, 0].reshape(seq_rows, -1)
    value_rows = returned[:, :, 1].reshape(seq_rows, -1)
    input_rows = jnp.dot(
        normed, input_projection_weight, preferred_element_type=jnp.float32
    ).astype(jnp.bfloat16)
    output_rows = jnp.dot(
        normed, output_projection_weight, preferred_element_type=jnp.float32
    ).astype(jnp.bfloat16)
    step_raw = jnp.dot(normed, step_projection_weight, preferred_element_type=jnp.float32)
    value_conv, next_value = short_conv(prior_values, value_rows, value_taps)
    input_conv, next_input = short_conv(prior_input_maps, input_rows, input_taps)
    output_conv, next_output = short_conv(prior_output_maps, output_rows, output_taps)
    timestep_size = jax.nn.softplus(step_raw + head_step_bias)
    step_decay = jnp.exp(-timestep_size * head_decay_rate + extra_log_decay)
    state_next, mixed_flat = state_step(
        recurrent_state,
        value_conv,
        input_conv,
        output_conv,
        timestep_size,
        step_decay,
        head_skip_gain,
    )
    mixer_rows = gated_norm(mixed_flat, gate_rows, group_norm_gain, D_INNER // GROUPS)
    partial_mix = jnp.dot(
        lax.all_gather(mixer_rows, "ep", axis=0, tiled=True),
        mixer_output_weight,
        preferred_element_type=jnp.float32,
    )
    mix_share = lax.psum_scatter(
        partial_mix.reshape(ep_count, seq_rows, -1).astype(jnp.bfloat16),
        "tp",
        scatter_dimension=1,
        tiled=True,
    )
    moved_mix = lax.all_to_all(mix_share, "ep", split_axis=0, concat_axis=2, tiled=True)
    mixed_out = lax.all_gather(moved_mix, "tp", axis=1, tiled=True).reshape(seq_rows, model_width)
    stream = (tokens.astype(jnp.float32) + mixed_out.astype(jnp.float32)).astype(jnp.bfloat16)
    ffn_rows = rms_scale(stream, expert_norm_gain).astype(jnp.bfloat16)
    shared_hidden = (
        jax.nn.silu(jnp.dot(ffn_rows, common_gate_weight, preferred_element_type=jnp.float32))
        * jnp.dot(ffn_rows, common_up_weight, preferred_element_type=jnp.float32)
    ).astype(jnp.bfloat16)
    shared_out = lax.psum(
        jnp.dot(shared_hidden, common_down_weight, preferred_element_type=jnp.float32).astype(
            jnp.bfloat16
        ),
        "tp",
    ).astype(jnp.float32)
    exp_local = routed_gate_weight.shape[0]
    expert_total = exp_local * ep_count
    topk_count = routes.shape[1]
    capacity = (seq_rows * topk_count + expert_total - 1) // expert_total + 1
    slot_count = expert_total * capacity
    expert_ids = jnp.arange(expert_total, dtype=jnp.int32)
    flat_routes = routes.reshape(-1)
    onehot = (flat_routes[:, None] == expert_ids[None, :]).astype(jnp.int32)
    slot_ids = jnp.sum((jnp.cumsum(onehot, axis=0) - onehot) * onehot, axis=1)
    positions = flat_routes * capacity + slot_ids
    matches = (jnp.arange(slot_count, dtype=jnp.int32)[:, None] == positions[None, :]).reshape(
        slot_count, seq_rows, topk_count
    )
    dispatch_mat = jnp.sum(matches.astype(jnp.float32), axis=2).astype(jnp.bfloat16)
    combine_mat = jnp.sum(jnp.where(matches, chosen_expert_weight[None], 0.0), axis=2)
    outgoing = jnp.dot(dispatch_mat, ffn_rows, preferred_element_type=jnp.float32).astype(
        jnp.bfloat16
    )
    outgoing = outgoing.reshape(ep_count, exp_local, capacity, model_width)
    half_width = model_width // tp_count
    own_cols = lax.dynamic_slice_in_dim(outgoing, tp_place * half_width, half_width, 3)
    full_rows = lax.all_gather(
        lax.all_to_all(own_cols, "ep", split_axis=0, concat_axis=0, tiled=True),
        "tp",
        axis=3,
        tiled=True,
    )
    partial_out = expert_partial(
        full_rows, routed_gate_weight, routed_up_weight, routed_down_weight
    )
    share_out = lax.psum_scatter(
        partial_out.astype(jnp.bfloat16), "tp", scatter_dimension=3, tiled=True
    )
    back_half = lax.all_to_all(share_out, "ep", split_axis=0, concat_axis=0, tiled=True)
    routed_half = lax.dot_general(
        combine_mat,
        back_half.reshape(slot_count, half_width).astype(jnp.float32),
        (((0,), (0,)), ((), ())),
        precision=lax.Precision.HIGHEST,
    )
    routed = lax.all_gather(routed_half.astype(jnp.bfloat16), "tp", axis=1, tiled=True).astype(
        routed_half.dtype
    )
    result = (stream.astype(jnp.float32) + shared_out + routed).astype(jnp.bfloat16)
    return (result, state_next, next_value, next_input, next_output)


def solution(mesh):
    return jax.shard_map(
        shards,
        mesh=mesh,
        in_specs=(
            P("ep", None),
            P(),
            P(None, "tp", "ep"),
            P(None, "tp", "ep"),
            P(None, "tp"),
            P(None, "tp"),
            P(None, "tp"),
            P("tp"),
            P("tp"),
            P("ep", "tp"),
            P(None, "tp"),
            P(None, "tp"),
            P(None, "tp"),
            P("ep", None, "tp"),
            P("ep", None, "tp"),
            P("ep", None, "tp"),
            P("tp"),
            P("tp"),
            P("tp", "ep"),
            P("ep", "tp", None, None),
            P(),
            P("ep", None),
            P("ep", None),
            P("ep", None, "tp"),
            P("ep", None, "tp"),
            P("ep", "tp", None),
            P(None, "tp"),
            P(None, "tp"),
            P("tp", None),
        ),
        out_specs=(
            P("ep", None),
            P("ep", "tp", None, None),
            P("ep", None, "tp"),
            P("ep", None, "tp"),
            P("ep", None, "tp"),
        ),
        check_vma=False,
    )
```

profile of v0, /device:TPU:0, one launch (start us, length us, event | category | flops | bytes accessed | tf_op | source)
XLA Modules:
  0.0 206.3 jit_solution(9300064261054911112)
XLA Ops:
  7.3 1.0 fusion.18
  8.3 0.8 fusion.20
  9.1 45.3 %all_gather.15 = bf16[128,2048]{1,0:T(8,128)(2,1)S(1)} all-gather(bf16[8,2048]{1,0:T(8,128)(2,1)S(1)} %fusion.20), channel_id=1, replica_groups=mesh['ep'=16,'tp'=2] {'ep'}, dimensions={0}, use_global_device_ids=true | all-gather | bytes 557056 | tf_op jit(solution)/shard_map/all_gather | solution.py:106
  54.5 2.2 %fusion.1 = bf16[16,8,256]{2,1,0:T(8,128)(2,1)} fusion(bf16[128,2048]{1,0:T(8,128)(2,1)S(1)} %all_gather.15, bf16[2048,128]{1,0:T(8,128)(2,1)} %bitcast.213, bf16[2048,128]{1,0:T(8,128)(2,1)} %bitcast.214), kind=kOutput, calls=%fused_computation.7 | convolution fusion | flops 136347648 | bytes 1638400 | tf_op jit(solution)/shard_map/dot_general | solution.py:105
  56.6 3.5 %all-to-all-start = ((bf16[16,8,256]{2,1,0:T(8,128)(2,1)}), bf16[16,8,256]{2,1,0:T(8,128)(2,1)S(1)}, u32[]{:S(2)}, u32[]{:S(2)}) async-start(bf16[16,8,256]{2,1,0:T(8,128)(2,1)} %fusion.1), calls=%async_computation | async-start | bytes 131072 | tf_op jit(solution)/shard_map/all_to_all | solution.py:110
  60.2 1.6 slice_reduce_fusion.3
  62.0 0.8 slice_convert_fusion.2
  62.8 0.1 reshape.313
  62.9 0.1 reshape.314
  63.0 0.1 reshape.315
  63.1 0.4 convolution_convert_fusion.7
  63.5 0.9 fusion.68
  64.3 0.8 multiply_bitcast_fusion.1
  65.1 2.0 convolution_convert_fusion.6
  67.2 0.7 mul.467
  67.9 0.1 eq.30
  68.1 0.2 select_reduce_fusion.1
  68.3 0.7 reduce_sum.82
  69.1 0.2 add_exponential_fusion
  69.3 0.9 slice_reduce_fusion.4
  70.1 1.0 fusion.65
  71.1 0.8 copy_convert_fusion
  71.9 0.1 reshape.316
  72.0 0.7 reshape.328
  72.7 0.7 broadcast_multiply_fusion
  73.4 9.4 %multiply_reduce_fusion = (f32[8,32,64]{2,1,0:T(8,128)S(1)}, f32[8,32,64,128]{3,2,1,0:T(8,128)}) fusion(f32[8,32,128]{2,1,0:T(8,128)S(1)} %get-tuple-element.41, f32[8,32,128]{2,1,0:T(8,128)S(1)} %get-tuple-element.42, f32[8,32,64]{2,1,0:T(8,128)S(1)} %get-tuple-element.15, f32[8,32,64,128]{3,2,1,0:T(8,128)} %param.48, f32[8,32]{1,0:T(8,128)S(1)} %get-tuple-element.35), kind=kLoop, calls=%fused_computation | loop fusion | flops 10469376 | bytes 17171456 | tf_op jit(solution)/shard_map/reduce_sum | solution.py:41
  82.8 0.1 reduce_sum.76
  82.9 1.2 multiply_reduce_fusion.1
  84.2 0.1 reduce_sum.79
  84.3 0.1 copy.108
  84.4 1.0 fusion.41
  85.4 44.1 %all_gather.16 = bf16[128,2048]{1,0:T(8,128)(2,1)S(1)} all-gather(bf16[8,2048]{1,0:T(8,128)(2,1)S(1)} %fusion.41), channel_id=1, replica_groups=mesh['ep'=16,'tp'=2] {'ep'}, dimensions={0}, use_global_device_ids=true | all-gather | bytes 557056 | tf_op jit(solution)/shard_map/all_gather | solution.py:138
  129.5 1.3 fusion.5
  130.8 0.6 copy.98
  131.5 0.7 multiply_add_fusion.1
  132.2 0.1 copy.102
  132.3 0.8 copy.103
  133.0 2.0 reduce-scatter.3.cloned.1.call-done
  135.1 1.3 copy.99
  136.4 6.7 %all-to-all-start.1 = ((bf16[16,4,128]{2,1,0:T(4,128)(2,1)}), bf16[16,4,128]{2,1,0:T(4,128)(2,1)S(1)}, u32[]{:S(2)}, u32[]{:S(2)}) async-start(bf16[16,4,128]{2,1,0:T(4,128)(2,1)} %copy.99), calls=%async_computation.2 | async-start | bytes 32768 | tf_op jit(solution)/shard_map/all_to_all | solution.py:148
  143.2 0.7 convert_reduce_fusion
  143.8 6.6 %all-to-all-done.1 = bf16[16,4,128]{2,1,0:T(4,128)(2,1)S(1)} async-done(((bf16[16,4,128]{2,1,0:T(4,128)(2,1)}), bf16[16,4,128]{2,1,0:T(4,128)(2,1)S(1)}, u32[]{:S(2)}, u32[]{:S(2)}) %all-to-all-start.1) | async-done | bytes 16416 | tf_op jit(solution)/shard_map/all_to_all | solution.py:148
  150.5 1.9 all_gather.17
  152.3 0.9 fusion.22
  153.2 0.6 copy-done.9
  153.8 1.0 convolution_convert_fusion.1
  154.8 0.8 reshape.306
  155.6 0.9 constant_dynamic-slice_fusion
  156.5 10.6 %all_to_all.44 = bf16[16,1,4,1024]{3,2,1,0:T(4,128)(2,1)S(1)} all-to-all(bf16[16,1,4,1024]{3,2,1,0:T(4,128)(2,1)S(1)} %constant_dynamic-slice_fusion), channel_id=1, replica_groups=mesh['ep'=16,'tp'=2] {'ep'}, dimensions={0} | all-to-all | bytes 262144 | tf_op jit(solution)/shard_map/all_to_all | solution.py:184
  167.2 2.0 all_gather.18
  169.2 2.2 %convolution_bitcast_fusion.1 = f32[16,1,4,256]{3,0,2,1:T(8,128)} fusion(bf16[1,2048,256]{2,1,0:T(8,128)(2,1)} %param.52, bf16[16,1,4,2048]{3,0,2,1:T(8,128)(2,1)S(1)} %all_gather.18), kind=kOutput, calls=%fused_computation.9 | convolution fusion | flops 67108864 | bytes 1376256 | tf_op jit(solution)/shard_map/slcd,ldf->slcf/dot_general | solution.py:55
  171.4 3.1 %fusion = bf16[16,1,4,2048]{3,0,2,1:T(8,128)(2,1)} fusion(bf16[1,256,2048]{2,1,0:T(8,128)(2,1)} %param.54, bf16[1,2048,256]{2,1,0:T(8,128)(2,1)} %param.53, bf16[16,1,4,2048]{3,0,2,1:T(8,128)(2,1)S(1)} %all_gather.18, f32[16,1,4,256]{3,0,2,1:T(8,128)} %convolution_bitcast_fusion.1), kind=kOutput, calls=%fused_computation.4 | convolution fusion | flops 134447104 | bytes 2686976 | tf_op jit(solution)/shard_map/slcf,lfd->slcd/dot_general | solution.py:58
  174.5 1.4 pad_maximum_fusion.1
  175.9 1.4 pad_maximum_fusion
  177.3 1.5 fusion.63
  178.8 1.0 reduce-scatter.5.cloned.1.call-done
  179.9 1.6 copy.106
  181.5 6.7 %all-to-all-start.3 = ((bf16[16,1,4,1024]{3,2,1,0:T(4,128)(2,1)}), bf16[16,1,4,1024]{3,2,1,0:T(4,128)(2,1)S(1)}, u32[]{:S(2)}, u32[]{:S(2)}) async-start(bf16[16,1,4,1024]{3,2,1,0:T(4,128)(2,1)} %copy.106), calls=%async_computation.5 | async-start | bytes 262144 | tf_op jit(solution)/shard_map/all_to_all | solution.py:195
  188.3 2.0 convolution_convert_fusion.2
  190.2 3.4 %psum.7 = bf16[8,2048]{1,0:T(8,128)(2,1)S(1)} all-reduce(bf16[8,2048]{1,0:T(8,128)(2,1)S(1)} %convolution_convert_fusion.2), channel_id=1, replica_groups=mesh['ep'=16,'tp'=2] {'tp'}, use_global_device_ids=true, to_apply=%region_6.7 | all-reduce | flops 16384 | bytes 65536 | tf_op jit(solution)/shard_map/psum | solution.py:156
  193.7 2.5 %all-to-all-done.3 = bf16[16,1,4,1024]{3,2,1,0:T(4,128)(2,1)S(1)} async-done(((bf16[16,1,4,1024]{3,2,1,0:T(4,128)(2,1)}), bf16[16,1,4,1024]{3,2,1,0:T(4,128)(2,1)S(1)}, u32[]{:S(2)}, u32[]{:S(2)}) %all-to-all-start.3) | async-done | bytes 131104 | tf_op jit(solution)/shard_map/all_to_all | solution.py:195
  196.2 0.8 convolution_convert_fusion.5
  197.1 1.8 all_gather.19
  198.9 0.6 fusion.26
  (53 shorter events, 1.1 us)
Async XLA Ops:
  7.2 55.9 %copy-start = (bf16[2048,512]{1,0:T(8,128)(2,1)S(1)}, bf16[2048,512]{1,0:T(8,128)(2,1)}, u32[]{:S(2)}) copy-start(bf16[2048,512]{1,0:T(8,128)(2,1)} %param.33) | copy-start | bytes 6291460
  7.2 59.9 %copy-start.8 = (f32[4,512]{1,0:T(4,128)S(1)}, f32[4,512]{1,0:T(4,128)}, u32[]{:S(2)}) copy-start(f32[4,512]{1,0:T(4,128)} %param.41) | copy-start | bytes 24580
  7.2 59.9 %copy-start.4 = (bf16[8,3,512]{2,0,1:T(8,128)(2,1)S(1)}, bf16[8,3,512]{2,0,1:T(8,128)(2,1)}, u32[]{:S(2)}) copy-start(bf16[8,3,512]{2,0,1:T(8,128)(2,1)} %param.44) | copy-start | bytes 73732
  7.2 60.0 %copy-start.11 = (f32[32]{0:T(128)S(1)}, f32[32]{0:T(128)}, u32[]{:S(2)}) copy-start(f32[32]{0:T(128)} %param.45) | copy-start | bytes 388
  7.2 60.7 %copy-start.7 = (s32[8,6]{1,0:T(8,128)S(1)}, s32[8,6]{1,0:T(8,128)}, u32[]{:S(2)}) copy-start(s32[8,6]{1,0:T(8,128)} %param.50) | copy-start | bytes 580
  7.2 61.8 %copy-start.3 = (bf16[2048,32]{0,1:T(8,128)(2,1)S(1)}, bf16[2048,32]{0,1:T(8,128)(2,1)}, u32[]{:S(2)}) copy-start(bf16[2048,32]{0,1:T(8,128)(2,1)} %param.35) | copy-start | bytes 393220
  7.2 61.8 %copy-start.13 = (f32[32]{0:T(128)S(1)}, f32[32]{0:T(128)}, u32[]{:S(2)}) copy-start(f32[32]{0:T(128)} %param.36) | copy-start | bytes 388
  7.2 61.8 %copy-start.12 = (f32[32]{0:T(128)S(1)}, f32[32]{0:T(128)}, u32[]{:S(2)}) copy-start(f32[32]{0:T(128)} %param.37) | copy-start | bytes 388
  7.3 61.8 %copy-start.10 = (f32[8,32]{1,0:T(8,128)S(1)}, f32[8,32]{1,0:T(8,128)}, u32[]{:S(2)}) copy-start(f32[8,32]{1,0:T(8,128)} %param.38) | copy-start | bytes 3076
  56.6 12.6 %all-to-all-start = ((bf16[16,8,256]{2,1,0:T(8,128)(2,1)}), bf16[16,8,256]{2,1,0:T(8,128)(2,1)S(1)}, u32[]{:S(2)}, u32[]{:S(2)}) async-start(bf16[16,8,256]{2,1,0:T(8,128)(2,1)} %fusion.1), calls=%async_computation | async-start | bytes 131072 | tf_op jit(solution)/shard_map/all_to_all | solution.py:110
  60.1 74.9 %reduce-scatter.3.cloned.1.call-start = ((), (), s32[]{:S(2)}) async-start(), calls=%async_computation.6 | async-start | bytes 49152 | tf_op jit(solution)/shard_map/reduce_scatter | solution.py:142
  67.1 1.3 copy-start.6
  73.4 11.0 %copy-start.2 = (bf16[8,3,2048]{2,0,1:T(8,128)(2,1)S(1)}, bf16[8,3,2048]{2,0,1:T(8,128)(2,1)}, u32[]{:S(2)}) copy-start(bf16[8,3,2048]{2,0,1:T(8,128)(2,1)} %param.42) | copy-start | bytes 294916
  73.4 80.4 %copy-start.5 = (f32[2048]{0:T(1024)S(1)}, f32[2048]{0:T(1024)}, u32[]{:S(2)}) copy-start(f32[2048]{0:T(1024)} %param.49) | copy-start | bytes 24580
  82.8 105.5 %copy-start.1 = (bf16[256,2048]{1,0:T(8,128)(2,1)S(1)}, bf16[256,2048]{1,0:T(8,128)(2,1)}, u32[]{:S(2)}) copy-start(bf16[256,2048]{1,0:T(8,128)(2,1)} %param.57) | copy-start | bytes 3145732
  136.4 14.0 %all-to-all-start.1 = ((bf16[16,4,128]{2,1,0:T(4,128)(2,1)}), bf16[16,4,128]{2,1,0:T(4,128)(2,1)S(1)}, u32[]{:S(2)}, u32[]{:S(2)}) async-start(bf16[16,4,128]{2,1,0:T(4,128)(2,1)} %copy.99), calls=%async_computation.2 | async-start | bytes 32768 | tf_op jit(solution)/shard_map/all_to_all | solution.py:148
  143.1 36.7 %reduce-scatter.5.cloned.1.call-start = ((), (), s32[]{:S(2)}) async-start(), calls=%async_computation.7 | async-start | bytes 393216 | tf_op jit(solution)/shard_map/reduce_scatter | solution.py:192
  153.2 0.6 copy-start.9
  181.5 14.7 %all-to-all-start.3 = ((bf16[16,1,4,1024]{3,2,1,0:T(4,128)(2,1)}), bf16[16,1,4,1024]{3,2,1,0:T(4,128)(2,1)S(1)}, u32[]{:S(2)}, u32[]{:S(2)}) async-start(bf16[16,1,4,1024]{3,2,1,0:T(4,128)(2,1)} %copy.106), calls=%async_computation.5 | async-start | bytes 262144 | tf_op jit(solution)/shard_map/all_to_all | solution.py:195
Sparse Core Ops, SparseCore 0:
  131.6 3.4 reduce-scatter.2
  174.6 5.2 reduce-scatter.4
where the time goes:
time: 208 us; the launch traced here: 206 us
  blocking collectives  109 us (52%)
  other arithmetic  23.6 us (11%)
  starting transfers between devices  17 us (8%)
  matrix products  16.5 us (8%)
  between operations  14.4 us (7%)
  local copies, waits for them, and re-layouts  13.5 us (6%)
  waiting for transfers between devices  12.3 us (6%)
    all_gather x1, blocking collectives, shards(): lax.all_gather(normed, 'ep', axis=0, tiled=True)  45.3 us
    all_gather x1, blocking collectives, shards(): lax.all_gather(mixer_rows, 'ep', axis=0, tiled=True)  44.1 us
    all_to_all x1, blocking collectives, shards(): lax.all_to_all(own_cols, 'ep', split_axis=0, concat_axis=0, tiled=True)  10.6 us
    reduce_sum x1, other arithmetic, state_step(): jnp.sum(state_next * output_heads[:, :, None, :], axis=-1)  9.36 us
    all_to_all x1, starting transfers between devices, shards(): lax.all_to_all(share_out, 'ep', split_axis=0, concat_axis=0, tiled=True)  6.73 us
    all_to_all x1, starting transfers between devices, shards(): lax.all_to_all(mix_share, 'ep', split_axis=0, concat_axis=2, tiled=True)  6.69 us
    all_to_all x1, waiting for transfers between devices, shards(): lax.all_to_all(mix_share, 'ep', split_axis=0, concat_axis=2, tiled=True)  6.62 us
  transfers between devices with their start and end apart: 5, of which 4 were waited for; matrix products, arithmetic and copies ran while one was open for 8% of the time, Pallas kernels for 0%

commit v1 on v0

v1 whole, which is shorter than its diff:
```python
import jax
import jax.numpy as jnp
from jax import lax
from jax.sharding import PartitionSpec as P

GROUP_COUNT = 8
EPSILON = 1e-06
BF = jnp.bfloat16
F32 = jnp.float32


def dotf(a, b):
    return jnp.dot(a, b, preferred_element_type=F32)


def rms_rows(rows):
    return lax.rsqrt(jnp.mean(rows * rows, axis=-1, keepdims=True) + EPSILON)


def conv_rows(past_rows, fresh_row, taps):
    summed = fresh_row.astype(F32) * taps[-1]
    for offset in range(past_rows.shape[1]):
        summed = summed + past_rows[:, offset].astype(F32) * taps[offset]
    return jax.nn.silu(summed)


def shards(
    tokens,
    mixer_norm_gain,
    gate_projection_weight,
    value_projection_weight,
    input_projection_weight,
    output_projection_weight,
    step_projection_weight,
    head_step_bias,
    head_decay_rate,
    extra_log_decay,
    value_taps,
    input_taps,
    output_taps,
    prior_values,
    prior_input_maps,
    prior_output_maps,
    head_skip_gain,
    group_norm_gain,
    mixer_output_weight,
    recurrent_state,
    expert_norm_gain,
    routes,
    chosen_expert_weight,
    routed_gate_weight,
    routed_up_weight,
    routed_down_weight,
    common_gate_weight,
    common_up_weight,
    common_down_weight,
):
    seqs, width = tokens.shape
    n_ep = lax.axis_size("ep")
    n_tp = lax.axis_size("tp")
    ep = lax.axis_index("ep")
    tp = lax.axis_index("tp")
    total = n_ep * seqs
    half = width // n_tp
    topk = routes.shape[1]
    heads, head_size, state_size = recurrent_state.shape[1:]
    channels = heads * head_size
    groups = input_projection_weight.shape[1] // state_size
    per_group = heads // groups

    def to_all(rows):
        wide = jnp.broadcast_to(rows[None], (n_ep,) + rows.shape)
        return lax.all_to_all(wide, "ep", split_axis=0, concat_axis=0, tiled=True)

    def swap(rows):
        return lax.ppermute(rows, "tp", [(i, (i + 1) % n_tp) for i in range(n_tp)])

    own_half = lax.dynamic_slice_in_dim(tokens, tp * half, half, 1)
    route_cols = jnp.pad(routes.astype(BF), ((0, 0), (0, 128 - topk)))
    halves = to_all(jnp.concatenate([own_half, route_cols], axis=1))
    all_routes = halves[:, :, half : half + topk].reshape(total, topk).astype(jnp.int32)
    tokens_all = lax.all_gather(
        halves[:, :, :half].reshape(total, half), "tp", axis=1, tiled=True
    ).astype(F32)

    own = tokens.astype(F32)
    normed = (own * rms_rows(own) * mixer_norm_gain).astype(BF)
    input_rows = dotf(normed, input_projection_weight).astype(BF)
    output_rows = dotf(normed, output_projection_weight).astype(BF)
    step_raw = dotf(normed, step_projection_weight)
    input_conv = conv_rows(prior_input_maps, input_rows, input_taps)
    output_conv = conv_rows(prior_output_maps, output_rows, output_taps)
    step_size = jax.nn.softplus(step_raw + head_step_bias)
    decay = jnp.exp(-step_size * head_decay_rate + extra_log_decay)
    input_g = input_conv.reshape(seqs, groups, state_size)
    output_g = output_conv.reshape(seqs, groups, state_size)
    input_heads = jnp.repeat(input_g, per_group, axis=1)
    output_heads = jnp.repeat(output_g, per_group, axis=1)
    map_dot = jnp.repeat(jnp.sum(input_g * output_g, axis=-1), per_group, axis=1)
    read_out = jnp.sum(recurrent_state * output_heads[:, :, None, :], axis=-1)
    base_rows = (decay[:, :, None] * read_out).reshape(seqs, channels)
    slope = step_size * map_dot + head_skip_gain

    def widen(per_head):
        return jnp.broadcast_to(per_head[:, :, None], (seqs, heads, head_size)).reshape(
            seqs, channels
        )

    slope_rows = widen(slope)

    normed_all = (tokens_all * rms_rows(tokens_all) * mixer_norm_gain).astype(BF)
    both = jnp.concatenate(
        [
            gate_projection_weight.reshape(width, -1),
            value_projection_weight.reshape(width, -1),
        ],
        axis=1,
    )
    piece = both.shape[1] // 2
    projected = dotf(normed_all, both).astype(BF).reshape(n_ep, seqs, 2 * piece)
    returned = lax.all_to_all(projected, "ep", split_axis=0, concat_axis=0, tiled=True)
    gate_rows = jnp.swapaxes(returned[:, :, :piece], 0, 1).reshape(seqs, channels)
    value_rows = jnp.swapaxes(returned[:, :, piece:], 0, 1).reshape(seqs, channels)

    value_conv = conv_rows(prior_values, value_rows, value_taps)
    mixed_flat = base_rows + slope_rows * value_conv
    gated = (mixed_flat * jax.nn.silu(gate_rows.astype(F32))).reshape(seqs, groups, -1)
    mixer_rows = (
        (gated * rms_rows(gated)).reshape(seqs, channels) * group_norm_gain
    ).astype(BF)

    rows_all = to_all(mixer_rows).reshape(total, channels)
    partial = dotf(rows_all, mixer_output_weight).astype(BF)
    block = total // n_tp
    mine = lax.dynamic_slice_in_dim(partial, tp * block, block, 0)
    other = lax.dynamic_slice_in_dim(partial, (n_tp - 1 - tp) * block, block, 0)
    summed = (mine.astype(F32) + swap(other).astype(F32)).astype(BF)
    mixed_all = lax.all_gather(to_all(summed), "tp", axis=1, tiled=True)
    mixed_all = jnp.swapaxes(mixed_all, 0, 1).reshape(total, width)

    stream_all = (tokens_all + mixed_all.astype(F32)).astype(BF)
    stream32 = stream_all.astype(F32)
    ffn_all = (stream32 * rms_rows(stream32) * expert_norm_gain).astype(BF)

    exp_local = routed_gate_weight.shape[0]
    experts = exp_local * n_ep
    cap = (seqs * topk + experts - 1) // experts + 1
    slots = jnp.arange(cap, dtype=jnp.int32)

    def dispatch(local):
        named = jnp.any(all_routes == ep * exp_local + local, axis=1).reshape(n_ep, seqs)
        place = jnp.cumsum(named.astype(jnp.int32), axis=1) - 1
        pick = named[:, None, :] & (place[:, None, :] == slots[None, :, None])
        eye = jnp.arange(n_ep)[:, None] == jnp.arange(n_ep)[None, :]
        return (
            (pick[:, :, None, :] & eye[:, None, :, None]).reshape(n_ep * cap, total).astype(BF)
        )

    outs = []
    for local in range(exp_local):
        picked = dotf(dispatch(local), ffn_all).astype(BF)
        hidden = (
            jax.nn.silu(dotf(picked, routed_gate_weight[local]))
            * dotf(picked, routed_up_weight[local])
        ).astype(BF)
        outs.append(dotf(hidden, routed_down_weight[local]).astype(BF))
    sent = jnp.stack([o.reshape(n_ep, cap, width) for o in outs], axis=1)
    back = lax.all_to_all(sent, "ep", split_axis=0, concat_axis=0, tiled=True)
    back = back.reshape(experts * cap, width)

    stream_own = lax.dynamic_slice_in_dim(stream_all, ep * seqs, seqs, 0)
    ffn_own = lax.dynamic_slice_in_dim(ffn_all, ep * seqs, seqs, 0)
    shared_hidden = (
        jax.nn.silu(dotf(ffn_own, common_gate_weight)) * dotf(ffn_own, common_up_weight)
    ).astype(BF)
    shared_part = dotf(shared_hidden, common_down_weight)
    expert_ids = jnp.arange(experts, dtype=jnp.int32)
    hit = routes[:, :, None] == expert_ids
    weight_of = jnp.sum(jnp.where(hit, chosen_expert_weight[:, :, None], 0.0), axis=1)
    named = jnp.any(hit, axis=1).astype(jnp.int32)
    place = jnp.cumsum(named, axis=0) - named
    combine = jnp.where(
        place[:, :, None] == slots[None, None, :], weight_of[:, :, None], 0.0
    ).reshape(seqs, experts * cap)
    routed_part = jnp.dot(combine, back.astype(F32), precision=lax.Precision.HIGHEST)
    part = (shared_part + routed_part).astype(BF)
    other_part = swap(part)
    result = (
        stream_own.astype(F32) + (part.astype(F32) + other_part.astype(F32))
    ).astype(BF)

    state_next = (
        decay[:, :, None, None] * recurrent_state
        + (step_size[:, :, None] * value_conv.reshape(seqs, heads, head_size))[..., None]
        * input_heads[:, :, None, :]
    )

    def shifted(past, fresh):
        return jnp.concatenate([past[:, 1:], fresh[:, None]], axis=1)

    return (
        result,
        state_next,
        shifted(prior_values, value_rows),
        shifted(prior_input_maps, input_rows),
        shifted(prior_output_maps, output_rows),
    )


def solution(mesh):
    return jax.shard_map(
        shards,
        mesh=mesh,
        in_specs=(
            P("ep", None),
            P(),
            P(None, "tp", "ep"),
            P(None, "tp", "ep"),
            P(None, "tp"),
            P(None, "tp"),
            P(None, "tp"),
            P("tp"),
            P("tp"),
            P("ep", "tp"),
            P(None, "tp"),
            P(None, "tp"),
            P(None, "tp"),
            P("ep", None, "tp"),
            P("ep", None, "tp"),
            P("ep", None, "tp"),
            P("tp"),
            P("tp"),
            P("tp", "ep"),
            P("ep", "tp", None, None),
            P(),
            P("ep", None),
            P("ep", None),
            P("ep", None, "tp"),
            P("ep", None, "tp"),
            P("ep", "tp", None),
            P(None, "tp"),
            P(None, "tp"),
            P("tp", None),
        ),
        out_specs=(
            P("ep", None),
            P("ep", "tp", None, None),
            P("ep", None, "tp"),
            P("ep", None, "tp"),
            P("ep", None, "tp"),
        ),
        check_vma=False,
    )
```

time: 208 us -> 129 us (0.62)
  blocking collectives: 109 us -> 4.36 us
  waiting for transfers between devices: 12.3 us -> 29.6 us
  between operations: 14.4 us -> 0.98 us
  starting transfers between devices: 17 us -> 26.5 us
  local copies, waits for them, and re-layouts: 13.5 us -> 22.2 us
  matrix products: 16.5 us -> 19.5 us
    all_gather x5 -> x2, blocking collectives: 95.1 us -> 4.36 us  [the longest x1 2.18 us: shards(): lax.all_gather(halves[:, :, :half].reshape(total, half), 'tp', axis=1, ti...]
    all_to_all x3 -> x5, waiting for transfers between devices: 9.14 us -> 28.5 us  [the longest x3 15 us: to_all(): return lax.all_to_all(wide, 'ep', split_axis=0, concat_axis=0, tiled=True)]
    all_to_all x1 -> x0, blocking collectives: 10.6 us -> none  [shards(): lax.all_to_all(own_cols, 'ep', split_axis=0, concat_axis=0, tiled=True)]
    reduce_sum x7, other arithmetic: 13.4 us -> 3.63 us  [the longest x5 1.96 us: rms_rows(): return lax.rsqrt(jnp.mean(rows * rows, axis=-1, keepdims=True) + EPSILON)]
    all_to_all x3 -> x5, starting transfers between devices: 16.9 us -> 26.3 us  [the longest x3 15.9 us: to_all(): return lax.all_to_all(wide, 'ep', split_axis=0, concat_axis=0, tiled=True)]
    add x1, other arithmetic: 0.7 us -> 9.4 us  [shards(): decay[:, :, None, None] * recurrent_state]
    psum x1 -> x0, blocking collectives: 3.41 us -> none  [shards(): lax.psum(jnp.dot(shared_hidden, common_down_weight, preferred_element_typ...]
    reduce_scatter x2 -> x0, waiting for transfers between devices: 3.09 us -> none  [the longest x1 2.04 us: shards(): lax.psum_scatter(partial_mix.reshape(ep_count, seq_rows, -1).astype(jnp.b...]
  transfers between devices with their start and end apart: 5 -> 7, of which waited for: 4 -> 6; matrix products, arithmetic and copies ran while one was open for 8% -> 25% of each run, Pallas kernels for 0% -> 0%
where the time goes in v1:
time: 129 us; the launch traced here: 127 us
  waiting for transfers between devices  29.6 us (23%)
  starting transfers between devices  26.5 us (21%)
  other arithmetic  23.7 us (18%)
  local copies, waits for them, and re-layouts  22.2 us (17%)
  matrix products  19.5 us (15%)
  blocking collectives  4.36 us (3%)
    dot_general x10, matrix products, dotf(): return jnp.dot(a, b, preferred_element_type=F32)  18.4 us
    all_to_all x3, starting transfers between devices, to_all(): return lax.all_to_all(wide, 'ep', split_axis=0, concat_axis=0, tiled=True)  15.9 us
    all_to_all x3, waiting for transfers between devices, to_all(): return lax.all_to_all(wide, 'ep', split_axis=0, concat_axis=0, tiled=True)  15 us
    add x1, other arithmetic, shards(): decay[:, :, None, None] * recurrent_state  9.4 us
    all_to_all x1, waiting for transfers between devices, shards(): lax.all_to_all(projected, 'ep', split_axis=0, concat_axis=0, tiled=True)  7.51 us
    all_to_all x1, starting transfers between devices, shards(): lax.all_to_all(projected, 'ep', split_axis=0, concat_axis=0, tiled=True)  6.91 us
    all_to_all x1, waiting for transfers between devices, shards(): back = lax.all_to_all(sent, 'ep', split_axis=0, concat_axis=0, tiled=True)  5.99 us
    all_to_all x1, starting transfers between devices, shards(): back = lax.all_to_all(sent, 'ep', split_axis=0, concat_axis=0, tiled=True)  3.56 us
  transfers between devices with their start and end apart: 7, of which 6 were waited for; matrix products, arithmetic and copies ran while one was open for 25% of the time, Pallas kernels for 0%

profile of v1, /device:TPU:0, one launch (start us, length us, event | category | flops | bytes accessed | tf_op | source)
XLA Modules:
  0.0 126.9 jit_solution(15633705970482824894)
XLA Ops:
  0.7 0.8 convert_element_type.270
  1.5 0.7 constant_dynamic-slice_fusion.1
  2.2 0.7 broadcast_in_dim.34
  3.0 8.3 %all-to-all-start = ((bf16[16,8,1152]{2,1,0:T(8,128)(2,1)}), bf16[16,8,1152]{2,1,0:T(8,128)(2,1)S(1)}, u32[]{:S(2)}, u32[]{:S(2)}) async-start(bf16[16,8,1152]{2,1,0:T(8,128)(2,1)} %broadcast_in_dim.34), calls=%async_computation | async-start | bytes 589824 | tf_op jit(solution)/shard_map/all_to_all | solution.py:73
  11.3 0.9 fusion.26
  12.2 1.2 convolution_convert_fusion.5
  13.4 2.0 %convolution_convert_fusion.4 = bf16[8,512]{1,0:T(8,128)(2,1)S(1)} fusion(bf16[2048,512]{1,0:T(8,128)(2,1)} %param.33, bf16[8,2048]{1,0:T(8,128)(2,1)} %param.29, f32[2048]{0:T(1024)} %param.30, f32[8]{0:T(128)S(1)} %add_rsqrt_fusion.3), kind=kOutput, calls=%fused_computation.16 | convolution fusion | flops 16846848 | bytes 2146336 | tf_op jit(solution)/shard_map/dot_general | solution.py:13
  15.4 0.9 fusion.78
  16.3 0.9 fusion.77
  17.2 0.9 multiply_reduce_fusion.2
  18.3 1.8 %add_exponential_fusion = (f32[8,32]{1,0:T(8,128)}, f32[8,32]{1,0:T(8,128)S(1)}, f32[8,32]{1,0:T(8,128)}) fusion(f32[8,32]{1,0:T(8,128)} %param.38, f32[32]{0:T(128)} %param.37, f32[32]{0:T(128)} %param.45, f32[8,32]{1,0:T(8,128)S(1)} %reshape.463, f32[32]{0:T(128)} %param.36, bf16[2048,32]{0,1:T(8,128)(2,1)} %param.35, bf16[8,2048]{1,0:T(8,128)(2,1)} %param.29, ...), kind=kOutput, calls=%fused_computation.126 | convolution fusion | flops 1117184 | bytes 177568 | tf_op jit(solution)/shard_map/dot_general | solution.py:13
  20.1 1.6 %slice_reduce_fusion.3 = (f32[2048]{0:T(1024)S(1)}, f32[2048]{0:T(1024)S(1)}, f32[2048]{0:T(1024)S(1)}, f32[2048]{0:T(1024)S(1)}, f32[1,2048]{1,0:T(1,128)}, /*i...) fusion(f32[4,2048]{1,0:T(4,128)} %param.39), kind=kLoop, calls=%fused_computation.142 | loop fusion | bytes 98304 | tf_op jit(solution)/shard_map/slice | solution.py:21
  21.7 0.7 mul.497
  22.4 0.7 mul.500
  23.0 0.7 mul.503
  23.7 0.7 mul.506
  24.5 0.7 reshape.464
  25.2 0.8 slice_convert_fusion.2
  26.1 0.7 reshape.483
  26.9 0.7 reshape.484
  27.6 2.2 %all_gather.6 = bf16[128,2048]{1,0:T(8,128)(2,1)S(1)} all-gather(bf16[128,1024]{1,0:T(8,128)(2,1)S(1)} %slice_bitcast_fusion), channel_id=1, replica_groups=mesh['ep'=16,'tp'=2] {'tp'}, dimensions={1}, use_global_device_ids=true | all-gather | bytes 786432 | tf_op jit(solution)/shard_map/all_gather | solution.py:82
  30.0 2.2 %fusion.1 = bf16[16,8,256]{2,1,0:T(8,128)(2,1)} fusion(bf16[2048,128]{1,0:T(8,128)(2,1)} %bitcast.182, bf16[2048,128]{1,0:T(8,128)(2,1)} %bitcast.183, bf16[128,2048]{1,0:T(8,128)(2,1)S(1)} %all_gather.6, f32[2048]{0:T(1024)S(1)} %copy-done.5, f32[128]{0:T(128)S(1)} %add_rsqrt_fusion.2), kind=kOutput, calls=%fused_computation.12 | convolution fusion | flops 137396224 | bytes 1647104 | tf_op jit(solution)/shard_map/dot_general | solution.py:13
  32.2 6.9 %all-to-all-start.1 = ((bf16[16,8,256]{2,1,0:T(8,128)(2,1)}), bf16[16,8,256]{2,1,0:T(8,128)(2,1)S(1)}, u32[]{:S(2)}, u32[]{:S(2)}) async-start(bf16[16,8,256]{2,1,0:T(8,128)(2,1)} %fusion.1), calls=%async_computation.1 | async-start | bytes 131072 | tf_op jit(solution)/shard_map/all_to_all | solution.py:121
  39.1 7.5 %all-to-all-done.1 = bf16[16,8,256]{2,1,0:T(8,128)(2,1)S(1)} async-done(((bf16[16,8,256]{2,1,0:T(8,128)(2,1)}), bf16[16,8,256]{2,1,0:T(8,128)(2,1)S(1)}, u32[]{:S(2)}, u32[]{:S(2)}) %all-to-all-start.1) | async-done | bytes 65568 | tf_op jit(solution)/shard_map/all_to_all | solution.py:121
  46.6 0.6 slice_bitcast_fusion.1
  47.3 0.6 copy.60
  47.9 1.6 %reshape.485 = f32[8,32,64]{2,1,0:T(8,128)} reshape(f32[8,16,128]{2,1,0:T(8,128)} %copy.60) | data formatting | bytes 131072 | tf_op jit(solution)/shard_map/convert_element_type | solution.py:127
  49.5 0.7 reshape.481
  50.2 1.2 broadcast_multiply_fusion
  51.5 9.4 %multiply_add_fusion = (f32[8,32,64,128]{3,2,1,0:T(8,128)}, f32[8,32,64]{2,1,0:T(8,128)S(1)}) fusion(f32[8,32,64,128]{3,2,1,0:T(8,128)} %param.48, f32[8,32,128]{2,1,0:T(8,128)S(1)} %get-tuple-element.41, f32[8,32,64]{2,1,0:T(8,128)S(1)} %get-tuple-element.9, f32[8,32]{1,0:T(8,128)} %get-tuple-element.38, f32[8,32,128]{2,1,0:T(8,128)S(1)} %get-tuple-element.42), kind=kLoop, calls=%fused_computation | loop fusion | flops 10469376 | bytes 17171456 | tf_op jit(solution)/shard_map/add | solution.py:193
  61.6 0.8 fusion.44
  62.4 0.8 broadcast_in_dim.38
  63.2 3.6 %all-to-all-start.2 = ((bf16[16,8,2048]{2,1,0:T(8,128)(2,1)}), bf16[16,8,2048]{2,1,0:T(8,128)(2,1)S(1)}, u32[]{:S(2)}, u32[]{:S(2)}) async-start(bf16[16,8,2048]{2,1,0:T(8,128)(2,1)} %broadcast_in_dim.38), calls=%async_computation.2 | async-start | bytes 1048576 | tf_op jit(solution)/shard_map/all_to_all | solution.py:73
  66.8 1.4 %copy.63 = s32[8,6]{0,1:T(8,128)} copy(s32[8,6]{1,0:T(8,128)} %param.50) | data formatting | bytes 384 | tf_op args[21]
  68.2 1.3 %slice.122 = bf16[8,2,512]{2,0,1:T(8,128)(2,1)} slice(bf16[8,3,512]{2,0,1:T(8,128)(2,1)} %param.43), slice={[0:8], [1:3], [0:512]} | slice | bytes 32768 | tf_op jit(solution)/shard_map/slice | solution.py:199
  69.5 1.3 %slice.123 = bf16[8,2,512]{2,0,1:T(8,128)(2,1)} slice(bf16[8,3,512]{2,0,1:T(8,128)(2,1)} %param.44), slice={[0:8], [1:3], [0:512]} | slice | bytes 32768 | tf_op jit(solution)/shard_map/slice | solution.py:199
  70.8 0.8 fusion.53
  71.7 0.8 copy.65
  72.5 0.8 select_reduce_fusion
  73.3 0.6 iota_compare_fusion.4
  73.9 1.4 %pad_maximum_fusion.1 = (bf16[8,3,512]{2,0,1:T(8,128)(2,1)}, bf16[8,3,512]{2,0,1:T(8,128)(2,1)}) fusion(bf16[8,1,512]{2,0,1:T(8,128)(2,1)S(1)} %bitcast.169, bf16[8,2,512]{2,0,1:T(8,128)(2,1)} %slice.122, bf16[8,1,512]{2,0,1:T(8,128)(2,1)S(1)} %bitcast.168, bf16[8,2,512]{2,0,1:T(8,128)(2,1)} %slice.123), kind=kLoop, calls=%fused_computation.95 | loop fusion | flops 24576 | bytes 98304 | tf_op jit(solution)/shard_map/concatenate | solution.py:199
  75.3 5.9 %all-to-all-done.2 = bf16[16,8,2048]{2,1,0:T(8,128)(2,1)S(1)} async-done(((bf16[16,8,2048]{2,1,0:T(8,128)(2,1)}), bf16[16,8,2048]{2,1,0:T(8,128)(2,1)S(1)}, u32[]{:S(2)}, u32[]{:S(2)}) %all-to-all-start.2) | async-done | bytes 524320 | tf_op jit(solution)/shard_map/all_to_all | solution.py:73
  81.2 1.3 %convolution_convert_fusion.3 = bf16[128,128]{1,0:T(8,128)(2,1)S(1)} fusion(bf16[2048,128]{1,0:T(8,128)(2,1)} %param.47, bf16[16,8,2048]{2,1,0:T(8,128)(2,1)S(1)} %all-to-all-done.2), kind=kOutput, calls=%fused_computation.15 | convolution fusion | flops 67125248 | bytes 1081344 | tf_op jit(solution)/shard_map/dot_general | solution.py:13
  82.6 0.4 fusion.43
  83.1 0.6 collective-permute-done
  83.8 0.7 broadcast_in_dim.39
  84.5 4.0 %all-to-all-start.3 = ((bf16[16,64,128]{2,1,0:T(8,128)(2,1)}), bf16[16,64,128]{2,1,0:T(8,128)(2,1)S(1)}, u32[]{:S(2)}, u32[]{:S(2)}) async-start(bf16[16,64,128]{2,1,0:T(8,128)(2,1)} %broadcast_in_dim.39), calls=%async_computation.3 | async-start | bytes 524288 | tf_op jit(solution)/shard_map/all_to_all | solution.py:73
  88.5 0.8 broadcast_and_fusion
  89.3 0.3 and.36
  89.6 9.1 %all-to-all-done.3 = bf16[16,64,128]{2,1,0:T(8,128)(2,1)S(1)} async-done(((bf16[16,64,128]{2,1,0:T(8,128)(2,1)}), bf16[16,64,128]{2,1,0:T(8,128)(2,1)S(1)}, u32[]{:S(2)}, u32[]{:S(2)}) %all-to-all-start.3) | async-done | bytes 262176 | tf_op jit(solution)/shard_map/all_to_all | solution.py:73
  98.9 2.2 %all_gather.7 = bf16[16,128,128]{2,0,1:T(8,128)(2,1)S(1)} all-gather(bf16[16,64,128]{2,0,1:T(8,128)(2,1)S(1)} %copy.62), channel_id=1, replica_groups=mesh['ep'=16,'tp'=2] {'tp'}, dimensions={1}, use_global_device_ids=true | all-gather | bytes 786432 | tf_op jit(solution)/shard_map/all_gather | solution.py:138
  101.1 0.6 fusion.5
  101.7 0.9 fusion.7
  102.9 2.1 %fusion.18 = f32[64,256]{1,0:T(8,128)} fusion(bf16[64,2048]{1,0:T(8,128)(2,1)S(1)} %convolution_convert_fusion.1, bf16[1,2048,256]{2,1,0:T(8,128)(2,1)} %param.52), kind=kOutput, calls=%fused_computation.34 | convolution fusion | flops 67108864 | bytes 1376256 | tf_op jit(solution)/shard_map/dot_general | solution.py:13
  105.0 3.1 %convolution_convert_fusion = bf16[64,2048]{1,0:T(8,128)(2,1)} fusion(bf16[64,2048]{1,0:T(8,128)(2,1)S(1)} %convolution_convert_fusion.1, bf16[1,256,2048]{2,1,0:T(8,128)(2,1)} %param.54, bf16[1,2048,256]{2,1,0:T(8,128)(2,1)} %param.53, f32[64,256]{1,0:T(8,128)} %fusion.18), kind=kOutput, calls=%fused_computation.2 | convolution fusion | flops 134447104 | bytes 2686976 | tf_op jit(solution)/shard_map/dot_general | solution.py:13
  108.1 1.8 %stack_reshape.3 = bf16[16,1,4,2048]{3,2,0,1:T(4,128)(2,1)} reshape(bf16[64,2048]{1,0:T(8,128)(2,1)} %convolution_convert_fusion) | data formatting | bytes 524288 | tf_op jit(solution)/shard_map/stack;reshape | solution.py:167
  109.8 3.6 %all-to-all-start.4 = ((bf16[16,1,4,2048]{3,2,1,0:T(4,128)(2,1)}), bf16[16,1,4,2048]{3,2,1,0:T(4,128)(2,1)S(1)}, u32[]{:S(2)}, u32[]{:S(2)}) async-start(bf16[16,1,4,2048]{3,2,1,0:T(4,128)(2,1)} %bitcast.165), calls=%async_computation.4 | async-start | bytes 524288 | tf_op jit(solution)/shard_map/all_to_all | solution.py:168
  113.4 1.5 %fusion.51 = f32[8,256]{1,0:T(8,128)S(1)} fusion(bf16[2048,256]{1,0:T(8,128)(2,1)} %param.55, bf16[128,2048]{1,0:T(8,128)(2,1)S(1)} %fusion.7, s32[]{:T(128)S(6)} %select_n.39), kind=kOutput, calls=%fused_computation.93 | convolution fusion | flops 8388608 | bytes 1089540 | tf_op jit(solution)/shard_map/dot_general | solution.py:13
  114.9 2.9 %fusion.4 = f32[8,2048]{1,0:T(8,128)} fusion(bf16[256,2048]{1,0:T(8,128)(2,1)} %param.57, bf16[2048,256]{1,0:T(8,128)(2,1)} %param.56, bf16[128,2048]{1,0:T(8,128)(2,1)S(1)} %fusion.7, s32[]{:T(128)S(6)} %select_n.39, f32[8,256]{1,0:T(8,128)S(1)} %fusion.51), kind=kOutput, calls=%fused_computation.20 | convolution fusion | flops 16789504 | bytes 2203652 | tf_op jit(solution)/shard_map/dot_general | solution.py:13
  117.8 6.0 %all-to-all-done.4 = bf16[16,1,4,2048]{3,2,1,0:T(4,128)(2,1)S(1)} async-done(((bf16[16,1,4,2048]{3,2,1,0:T(4,128)(2,1)}), bf16[16,1,4,2048]{3,2,1,0:T(4,128)(2,1)S(1)}, u32[]{:S(2)}, u32[]{:S(2)}) %all-to-all-start.4) | async-done | bytes 262176 | tf_op jit(solution)/shard_map/all_to_all | solution.py:168
  123.8 1.1 fusion
  125.1 0.7 pad_maximum_fusion
  125.7 0.5 collective-permute-done.1
  126.2 0.6 add_convert_fusion
  (61 shorter events, 2.5 us)
Async XLA Ops:
  0.6 11.6 %copy-start = (bf16[2048,512]{1,0:T(8,128)(2,1)S(1)}, bf16[2048,512]{1,0:T(8,128)(2,1)}, u32[]{:S(2)}) copy-start(bf16[2048,512]{1,0:T(8,128)(2,1)} %param.34) | copy-start | bytes 6291460
  0.6 29.4 %copy-start.5 = (f32[2048]{0:T(1024)S(1)}, f32[2048]{0:T(1024)}, u32[]{:S(2)}) copy-start(f32[2048]{0:T(1024)} %param.30) | copy-start | bytes 24580
  3.0 24.6 %all-to-all-start = ((bf16[16,8,1152]{2,1,0:T(8,128)(2,1)}), bf16[16,8,1152]{2,1,0:T(8,128)(2,1)S(1)}, u32[]{:S(2)}, u32[]{:S(2)}) async-start(bf16[16,8,1152]{2,1,0:T(8,128)(2,1)} %broadcast_in_dim.34), calls=%async_computation | async-start | bytes 589824 | tf_op jit(solution)/shard_map/all_to_all | solution.py:73
  20.1 4.4 %copy-start.7 = (f32[8,32]{1,0:T(8,128)}, f32[8,32]{1,0:T(8,128)S(1)}, u32[]{:S(2)}) copy-start(f32[8,32]{1,0:T(8,128)S(1)} %get-tuple-element.39) | copy-start | bytes 3076
  32.2 14.4 %all-to-all-start.1 = ((bf16[16,8,256]{2,1,0:T(8,128)(2,1)}), bf16[16,8,256]{2,1,0:T(8,128)(2,1)S(1)}, u32[]{:S(2)}, u32[]{:S(2)}) async-start(bf16[16,8,256]{2,1,0:T(8,128)(2,1)} %fusion.1), calls=%async_computation.1 | async-start | bytes 131072 | tf_op jit(solution)/shard_map/all_to_all | solution.py:121
  51.4 9.5 %copy-start.2 = (f32[8,32,64]{2,1,0:T(8,128)S(1)}, f32[8,32,64]{2,1,0:T(8,128)}, u32[]{:S(2)}) copy-start(f32[8,32,64]{2,1,0:T(8,128)} %reshape.485) | copy-start | bytes 196612
  51.4 9.4 %copy-start.6 = (f32[8,32]{1,0:T(8,128)S(1)}, f32[8,32]{1,0:T(8,128)}, u32[]{:S(2)}) copy-start(f32[8,32]{1,0:T(8,128)} %get-tuple-element.38) | copy-start | bytes 3076
  51.4 9.4 %copy-start.8 = (f32[8,32]{1,0:T(8,128)S(1)}, f32[8,32]{1,0:T(8,128)}, u32[]{:S(2)}) copy-start(f32[8,32]{1,0:T(8,128)} %copy-done.7) | copy-start | bytes 3076
  51.5 10.1 %copy-start.1 = (bf16[8,3,2048]{2,0,1:T(8,128)(2,1)S(1)}, bf16[8,3,2048]{2,0,1:T(8,128)(2,1)}, u32[]{:S(2)}) copy-start(bf16[8,3,2048]{2,0,1:T(8,128)(2,1)} %param.42) | copy-start | bytes 294916
  51.5 10.1 %copy-start.3 = (f32[8,2048]{1,0:T(8,128)S(1)}, f32[8,2048]{1,0:T(8,128)}, u32[]{:S(2)}) copy-start(f32[8,2048]{1,0:T(8,128)} %reshape.464) | copy-start | bytes 196612
  63.2 17.9 %all-to-all-start.2 = ((bf16[16,8,2048]{2,1,0:T(8,128)(2,1)}), bf16[16,8,2048]{2,1,0:T(8,128)(2,1)S(1)}, u32[]{:S(2)}, u32[]{:S(2)}) async-start(bf16[16,8,2048]{2,1,0:T(8,128)(2,1)} %broadcast_in_dim.38), calls=%async_computation.2 | async-start | bytes 1048576 | tf_op jit(solution)/shard_map/all_to_all | solution.py:73
  82.5 1.2 collective-permute-start
  84.5 40.5 %slice-start = ((bf16[8,3,2048]{2,0,1:T(8,128)(2,1)}), bf16[8,2,2048]{2,0,1:T(8,128)(2,1)S(1)}, s32[]{:S(2)}) async-start(bf16[8,3,2048]{2,0,1:T(8,128)(2,1)} %param.42), calls=%async_computation.5 | async-start | bytes 131072 | tf_op jit(solution)/shard_map/slice | solution.py:199
  84.5 40.5 %copy-start.4 = (bf16[8,1,2048]{2,0,1:T(8,128)(2,1)S(1)}, bf16[8,1,2048]{2,0,1:T(8,128)(2,1)}, u32[]{:S(2)}) copy-start(bf16[8,1,2048]{2,0,1:T(8,128)(2,1)} %get-tuple-element.23) | copy-start | bytes 98308
  84.5 14.2 %all-to-all-start.3 = ((bf16[16,64,128]{2,1,0:T(8,128)(2,1)}), bf16[16,64,128]{2,1,0:T(8,128)(2,1)S(1)}, u32[]{:S(2)}, u32[]{:S(2)}) async-start(bf16[16,64,128]{2,1,0:T(8,128)(2,1)} %broadcast_in_dim.39), calls=%async_computation.3 | async-start | bytes 524288 | tf_op jit(solution)/shard_map/all_to_all | solution.py:73
  109.8 13.9 %all-to-all-start.4 = ((bf16[16,1,4,2048]{3,2,1,0:T(4,128)(2,1)}), bf16[16,1,4,2048]{3,2,1,0:T(4,128)(2,1)S(1)}, u32[]{:S(2)}, u32[]{:S(2)}) async-start(bf16[16,1,4,2048]{3,2,1,0:T(4,128)(2,1)} %bitcast.165), calls=%async_computation.4 | async-start | bytes 524288 | tf_op jit(solution)/shard_map/all_to_all | solution.py:168
  125.0 1.3 %collective-permute-start.1 = (bf16[8,2048]{1,0:T(8,128)(2,1)S(1)}, bf16[8,2048]{1,0:T(8,128)(2,1)S(1)}, u32[]{:S(2)}, u32[]{:S(2)}) collective-permute-start(bf16[8,2048]{1,0:T(8,128)(2,1)S(1)} %fusion), channel_id=1, source_target_pairs={{0,1},{1,0},{2,3},{3,2},{4,5},{5,4},{6,7},{7,6},{8,9},{9,8},{10,11... | collective-permute-start | bytes 98312 | tf_op jit(solution)/shard_map/ppermute | solution.py:76
